TPU v7x, 256 devices: a whole 4x4x8 slice. The times are simulated.
256 devices in a mesh: sp: 16 (over y, x), tp: 16 (over z, core).
Axes of the slice: x: 4, y: 4, z: 8, core: 2. Of those that a mesh axis runs over, the one named last changes fastest.
Arguments:
- queries: bfloat16 [16384, 1536], P('sp', 'tp'), may hold values from -34 to 34
- latent: bfloat16 [16384, 512], P('sp'), may hold values from -6 to 6
- rot_key: bfloat16 [16384, 32], P('sp'), may hold values from -34 to 34
- latent_gain: float32 [512], replicated, may hold values from 0.1 to 1.9
- key_up: bfloat16 [512, 1024], P(None, 'tp'), may hold values from -0.25 to 0.25
- value_up: bfloat16 [512, 1024], P(None, 'tp'), may hold values from -0.70710678 to 0.70710678
- query_gain: float32 [96], replicated, may hold values from 0.5 to 6
- key_gain: float32 [96], replicated, may hold values from 0.5 to 6
- out_gain: float32 [1024], replicated, may hold values from 0.1 to 1.9
- out_weight: bfloat16 [1024, 2048], replicated, may hold values from -0.1875 to 0.1875
- residual: bfloat16 [16384, 2048], P(('sp', 'tp')), may hold values from -6 to 6
- ffn_gain: float32 [2048], replicated, may hold values from 0.1 to 1.9
- routes: int32 [16384, 2], P(('sp', 'tp')), may hold values from 0 to 15, all different within a row; in each aligned block of 64 rows (0 to 63, 64 to 127, ...) at most 9 rows name the same one
- route_weights: float32 [16384, 2], P(('sp', 'tp')), may hold values from 0.2 to 1
- expert_gate: bfloat16 [16, 2048, 2048], P('sp', None, 'tp'), may hold values from -0.125 to 0.125
- expert_up: bfloat16 [16, 2048, 2048], P('sp', None, 'tp'), may hold values from -0.125 to 0.125
- expert_down: bfloat16 [16, 2048, 2048], P('sp', 'tp'), may hold values from -0.125 to 0.125
Outputs:
- layer_out: bfloat16 [16384, 2048], P(('sp', 'tp'))
Inputs may be any that keep to these rules, and one draw needn't show every extreme that they name: `routes`: the 2 experts of a token differ. Among the 64 rows of one device each expert is named by at most 9 rows, a bound that some block reaches.
All inputs are finite; a program needn't handle non-finite values.
Results may differ from a plain program's by a relative error of at most 0.02.
The roundings to bfloat16 on the way count: a program that leaves them out, or rounds other values in their place, can miss the bound.
Values may be sent and summed in bfloat16 or wider, within the bound.
A program may use at most 128 MiB of HBM per device.

v0:
```python
import jax
import jax.numpy as jnp
from jax import lax
from jax.sharding import PartitionSpec as P

D = 2048
NOPE = 64
ROPE = 32
VH = 64
TOPK = 2
QK = 96
epsilon = 1e-06
rope_base = 10000.0


def rms_scale(values):
    return lax.rsqrt(jnp.mean(values * values, axis=-1, keepdims=True) + epsilon)


def rotate_half(values, angles):
    half_dims = values.shape[-1] // 2
    first_half = values[..., :half_dims]
    second_half = values[..., half_dims:]
    cosine = jnp.cos(angles)
    sine_val = jnp.sin(angles)
    return jnp.concatenate(
        [
            first_half * cosine - second_half * sine_val,
            second_half * cosine + first_half * sine_val,
        ],
        axis=-1,
    )


def head_prepare(raw_rows, gain_vec, angles):
    normed_rows = raw_rows * rms_scale(raw_rows) * gain_vec
    turned_rows = rotate_half(normed_rows[..., NOPE:], angles[:, None, :])
    return jnp.concatenate([normed_rows[..., :NOPE], turned_rows], axis=-1).astype(jnp.bfloat16)


def slot_targets(route_rows, expert_total, slot_cap):
    flat_routes = route_rows.reshape(-1)
    one_hot = (flat_routes[:, None] == jnp.arange(expert_total, dtype=jnp.int32)[None, :]).astype(
        jnp.int32
    )
    earlier = jnp.cumsum(one_hot, axis=0) - one_hot
    rank_in = jnp.sum(earlier * one_hot, axis=1)
    return (flat_routes * slot_cap + rank_in).reshape(route_rows.shape)


def select_matrix(targets, slot_total):
    hits = targets[:, :, None] == jnp.arange(slot_total, dtype=jnp.int32)[None, None, :]
    return jnp.sum(hits.astype(jnp.bfloat16), axis=1)


def shards(
    queries,
    latent,
    rot_key,
    latent_gain,
    key_up,
    value_up,
    query_gain,
    key_gain,
    out_gain,
    out_weight,
    residual,
    ffn_gain,
    routes,
    route_weights,
    expert_gate,
    expert_up,
    expert_down,
):
    shard_len = queries.shape[0]
    local_heads = key_up.shape[1] // NOPE
    sp_count = lax.axis_size("sp")
    tp_count = lax.axis_size("tp")
    my_first = lax.axis_index("sp") * shard_len
    my_last = my_first + shard_len - 1
    positions = my_first + jnp.arange(shard_len, dtype=jnp.int32)
    inverse = rope_base ** (-jnp.arange(0, ROPE, 2, dtype=jnp.float32) / ROPE)
    angles = positions.astype(jnp.float32)[:, None] * inverse[None, :]
    lat_f32 = latent.astype(jnp.float32)
    normed_latent = (lat_f32 * rms_scale(lat_f32) * latent_gain).astype(jnp.bfloat16)
    key_nope = jnp.dot(normed_latent, key_up, preferred_element_type=jnp.float32).astype(
        jnp.bfloat16
    )
    value_rows = jnp.dot(normed_latent, value_up, preferred_element_type=jnp.float32).astype(
        jnp.bfloat16
    )
    shared = rot_key.astype(jnp.float32)[:, None, :]
    raw_keys = jnp.concatenate(
        [key_nope.astype(jnp.float32).reshape(shard_len, local_heads, NOPE), shared], axis=-1
    )
    key_rows = head_prepare(raw_keys, key_gain, angles)
    query_rows = head_prepare(
        queries.astype(jnp.float32).reshape(shard_len, local_heads, QK), query_gain, angles
    )
    query_heads = jnp.transpose(query_rows, (1, 0, 2))
    bundle = jnp.concatenate(
        [
            jnp.transpose(key_rows, (1, 2, 0)),
            jnp.transpose(value_rows.reshape(shard_len, local_heads, VH), (1, 2, 0)),
        ],
        axis=1,
    )
    score_scale = QK ** (-0.5)
    init_state = (
        jnp.full((local_heads, shard_len), -1e30, jnp.float32),
        jnp.zeros((local_heads, shard_len), jnp.float32),
        jnp.zeros((local_heads, shard_len, VH), jnp.float32),
    )
    key_piece = lax.all_gather(bundle, "sp", axis=2, tiled=True)
    block_count = key_piece.shape[2] // shard_len

    def one_block(block_index, running_state):
        first_key = block_index * shard_len

        def compute(inner):
            row_peak, row_total, weighted = inner
            key_part = lax.dynamic_slice_in_dim(key_piece, block_index * shard_len, shard_len, 2)
            scores = (
                jnp.einsum(
                    "hqc,hck->hqk",
                    query_heads,
                    key_part[:, :QK, :],
                    preferred_element_type=jnp.float32,
                )
                * score_scale
            )
            key_pos = first_key + jnp.arange(shard_len, dtype=jnp.int32)
            allowed = key_pos[None, None, :] <= positions[None, :, None]
            scores = jnp.where(allowed, scores, -1e30)
            new_peak = jnp.maximum(row_peak, jnp.max(scores, axis=2))
            exponent = jnp.where(allowed, jnp.exp(scores - new_peak[..., None]), 0.0)
            factor = jnp.exp(row_peak - new_peak)
            new_total = row_total * factor + jnp.sum(exponent, axis=2)
            contrib = jnp.einsum(
                "hqk,hvk->hqv",
                exponent.astype(jnp.bfloat16),
                key_part[:, QK:, :],
                preferred_element_type=jnp.float32,
            )
            return (new_peak, new_total, weighted * factor[..., None] + contrib)

        return lax.cond(first_key <= my_last, compute, lambda inner: inner, running_state)

    row_peak, row_total, weighted = lax.fori_loop(0, block_count, one_block, init_state)
    attended = (weighted / row_total[..., None]).astype(jnp.bfloat16)
    tok_count = residual.shape[0]
    head_major = jnp.transpose(attended, (1, 0, 2)).reshape(shard_len, local_heads * VH)
    token_rows = lax.all_to_all(head_major, "tp", split_axis=0, concat_axis=1, tiled=True).astype(
        jnp.float32
    )
    normed_rows = (token_rows * rms_scale(token_rows) * out_gain).astype(jnp.bfloat16)
    partials = jnp.einsum(
        "tgc,gcd->tgd",
        normed_rows.reshape(tok_count, tp_count, -1),
        out_weight.reshape(tp_count, -1, D),
        preferred_element_type=jnp.float32,
    )
    rounded = lax.optimization_barrier(partials.astype(jnp.bfloat16))
    mixed = jnp.sum(rounded.astype(jnp.float32), axis=1)
    middle = residual.astype(jnp.float32) + mixed
    ffn_input = (middle * rms_scale(middle) * ffn_gain).astype(jnp.bfloat16)
    slot_cap = max(2, 9 * tok_count * TOPK // (8 * sp_count))
    slot_total = sp_count * slot_cap
    targets = slot_targets(routes, sp_count, slot_cap)
    chooser = select_matrix(targets, slot_total)
    outbound = (
        jnp.einsum("ts,td->sd", chooser, ffn_input, preferred_element_type=jnp.float32)
        .astype(jnp.bfloat16)
        .reshape(sp_count, slot_cap, D)
    )
    arrived = lax.all_to_all(outbound, "sp", split_axis=0, concat_axis=0, tiled=True)
    item_count = arrived.shape[1]
    flat_rows = arrived.reshape(sp_count * item_count, D)
    row_block = lax.all_gather(flat_rows, "tp", axis=0, tiled=True)
    gate_pre = jnp.dot(row_block, expert_gate[0], preferred_element_type=jnp.float32)
    up_pre = jnp.dot(row_block, expert_up[0], preferred_element_type=jnp.float32)
    hidden = (jax.nn.silu(gate_pre) * up_pre).astype(jnp.bfloat16)
    served = lax.psum_scatter(
        jnp.dot(hidden, expert_down[0], preferred_element_type=jnp.float32).astype(jnp.bfloat16),
        "tp",
        scatter_dimension=0,
        tiled=True,
    ).reshape(sp_count, item_count, D)
    returned_rows = lax.all_to_all(served, "sp", split_axis=0, concat_axis=0, tiled=True).reshape(
        slot_total, D
    )
    picked = (
        jnp.take(returned_rows, targets.reshape(-1), axis=0)
        .reshape(tok_count, TOPK, D)
        .astype(jnp.float32)
    )
    moe_sum = jnp.sum(picked * route_weights[:, :, None], axis=1)
    return (middle + moe_sum).astype(jnp.bfloat16)


def solution(mesh):
    return jax.shard_map(
        shards,
        mesh=mesh,
        in_specs=(
            P("sp", "tp"),
            P("sp", None),
            P("sp", None),
            P(),
            P(None, "tp"),
            P(None, "tp"),
            P(),
            P(),
            P(),
            P(),
            P(("sp", "tp"), None),
            P(),
            P(("sp", "tp"), None),
            P(("sp", "tp"), None),
            P("sp", None, "tp"),
            P("sp", None, "tp"),
            P("sp", "tp", None),
        ),
        out_specs=P(("sp", "tp"), None),
        check_vma=False,
    )
```

profile of v0, /device:TPU:97, one launch (start us, length us, event | category | flops | bytes accessed | tf_op | source)
XLA Modules:
  0.0 451.1 jit_solution(6509418621641927697)
XLA Ops:
  6.6 1.6 fusion.21
  8.3 1.8 fusion.29
  10.1 0.9 fusion.40
  11.0 1.0 fusion.42
  12.0 1.0 fusion.41
  13.0 0.6 fusion.30
  13.7 0.3 fusion.74
  14.1 0.7 pad_maximum_fusion
  14.9 0.2 copy.34
  15.2 0.1 reshape.499
  15.5 0.2 reduce_window_sum.11
  15.7 0.2 select_reduce_fusion
  15.8 0.1 reduce_sum.105
  16.1 61.9 %all-gather.3.cloned.1.call-done = bf16[1,160,16384]{2,1,0:T(8,128)(2,1)} async-done(((bf16[1,160,1024]{2,1,0:T(8,128)(2,1)}), bf16[1,160,16384]{2,1,0:T(8,128)(2,1)}) %all-gather.3.cloned.1.call-update) | async-done | bytes 5242896 | tf_op jit(solution)/shard_map/all_gather | solution.py:114
  78.0 9.9 %while.18 = (s32[]{:T(128)}, f32[1,1024]{1,0:T(1,128)S(1)}, f32[1,1024]{1,0:T(1,128)S(1)}, f32[1,1024,64]{1,2,0:T(8,128)S(1)}, s32[]{:T(128)}, /*index=5*/bf16[1...) while((s32[]{:T(128)}, f32[1,1024]{1,0:T(1,128)S(1)}, ...), condition=%wide.region_8.9_spmd.clone, body=%wide.region_3.8_spmd.clone.sunk | while | flops 352456704 | bytes 30515560 | solution.py:149
  78.0 9.1 %conditional.3 = ((f32[1,1024]{1,0:T(1,128)S(1)}, f32[1,1024]{1,0:T(1,128)S(1)}, f32[1,1024,64]{1,2,0:T(8,128)S(1)})) conditional(s32[]{:T(128)} %convert_element_type.207, (f32[1,1024]{1,0:T(1,128)S(1)}, f32[1,1024]{1,0:T(1,128)S(1)}, f32[1,1024,64]{1,2,0:T(8,128)S(1)}) %tuple.54, (s32[]{:T(128)}, s32[]{:T(128)}, s32[]{:T(128)}, ...), branch_computations={%region_4.0_spmd, %region_5.7_spmd} | conditional | flops 352456704 | bytes 30511242 | solution.py:147
  78.0 2.0 fusion.2
  80.1 2.0 copy-done.1
  82.1 1.5 fusion.4
  83.7 3.5 fusion.10
  87.9 0.2 copy.41
  88.1 0.9 reshape.512
  89.0 7.8 %all-to-all-start = ((bf16[16,2,2048]{2,1,0:T(2,128)(2,1)}), bf16[16,2,2048]{2,1,0:T(2,128)(2,1)S(1)}, u32[]{:S(2)}, u32[]{:S(2)}) async-start(bf16[16,2,2048]{2,1,0:T(2,128)(2,1)} %reshape.512), calls=%async_computation | async-start | bytes 262144 | tf_op jit(solution)/shard_map/all_to_all | solution.py:153
  96.9 6.2 %all-to-all-done = bf16[16,2,2048]{2,1,0:T(2,128)(2,1)S(1)} async-done(((bf16[16,2,2048]{2,1,0:T(2,128)(2,1)}), bf16[16,2,2048]{2,1,0:T(2,128)(2,1)S(1)}, u32[]{:S(2)}, u32[]{:S(2)}) %all-to-all-start) | async-done | bytes 131104 | tf_op jit(solution)/shard_map/all_to_all | solution.py:153
  103.1 0.2 reshape.513
  103.3 0.2 fusion.32
  103.5 3.5 convert_bitcast_fusion
  107.1 0.8 convert_reduce_fusion
  107.8 0.2 copy-done.2
  108.0 0.2 multiply_reduce_fusion.1
  108.2 0.4 convolution_convert_fusion.1
  108.5 0.2 reshape.500
  108.8 156.9 %all_to_all.23 = bf16[16,9,2048]{2,1,0:T(8,128)(2,1)S(1)} all-to-all(bf16[16,9,2048]{2,1,0:T(8,128)(2,1)S(1)} %reshape.500), channel_id=1, replica_groups=mesh['sp'=16,'tp'=16] {'sp'}, dimensions={0} | all-to-all | bytes 1179648 | tf_op jit(solution)/shard_map/all_to_all | solution.py:176
  265.7 1.1 reshape.501
  266.8 0.2 reduce-scatter.2.cloned.1.call-start
  267.1 57.2 %all-gather.5.cloned.1.call-done = bf16[2304,2048]{1,0:T(8,128)(2,1)} async-done(((bf16[144,2048]{1,0:T(8,128)(2,1)}), bf16[2304,2048]{1,0:T(8,128)(2,1)}) %all-gather.5.cloned.1.call-update) | async-done | bytes 9437200 | tf_op jit(solution)/shard_map/all_gather | solution.py:179
  324.3 5.3 %fusion.38 = f32[2304,128]{1,0:T(8,128)S(1)} fusion(bf16[2304,2048]{1,0:T(8,128)(2,1)} %all-gather.5.cloned.1.call-done, bf16[1,2048,128]{2,1,0:T(8,128)(2,1)} %param.35), kind=kOutput, calls=%fused_computation.53 | convolution fusion | flops 1207959552 | bytes 11141120 | tf_op jit(solution)/shard_map/dot_general | solution.py:180
  329.6 14.2 %convolution_convert_fusion = bf16[2304,2048]{1,0:T(8,128)(2,1)} fusion(bf16[2304,2048]{1,0:T(8,128)(2,1)} %all-gather.5.cloned.1.call-done, f32[2304,128]{1,0:T(8,128)S(1)} %fusion.38, bf16[1,128,2048]{2,1,0:T(8,128)(2,1)S(1)} %copy-done, bf16[1,2048,128]{2,1,0:T(8,128)(2,1)S(1)} %copy-done.5), kind=kOutput, calls=%fused_computation.23 | convolution fusion | flops 2422407168 | bytes 21102592 | tf_op jit(solution)/shard_map/dot_general | solution.py:184
  343.9 71.6 %reduce-scatter.2.cloned.1.call-done = bf16[144,2048]{1,0:T(8,128)(2,1)} async-done(((bf16[2304,2048]{1,0:T(8,128)(2,1)}), bf16[144,2048]{1,0:T(8,128)(2,1)}) %reduce-scatter.2.cloned.1.call-update) | async-done | bytes 589840 | tf_op jit(solution)/shard_map/reduce_scatter | solution.py:183
  415.5 2.3 reshape.502
  417.8 6.5 %all-to-all-start.2 = ((bf16[16,9,2048]{2,1,0:T(8,128)(2,1)}), bf16[16,9,2048]{2,1,0:T(8,128)(2,1)S(1)}, u32[]{:S(2)}, u32[]{:S(2)}) async-start(bf16[16,9,2048]{2,1,0:T(8,128)(2,1)} %reshape.502), calls=%async_computation.3 | async-start | bytes 2097152 | tf_op jit(solution)/shard_map/all_to_all | solution.py:189
  424.4 0.1 mul.304
  424.8 15.1 %all-to-all-done.2 = bf16[16,9,2048]{2,1,0:T(8,128)(2,1)S(1)} async-done(((bf16[16,9,2048]{2,1,0:T(8,128)(2,1)}), bf16[16,9,2048]{2,1,0:T(8,128)(2,1)S(1)}, u32[]{:S(2)}, u32[]{:S(2)}) %all-to-all-start.2) | async-done | bytes 589856 | tf_op jit(solution)/shard_map/all_to_all | solution.py:189
  439.9 0.3 reshape.503
  440.2 0.9 gather_fusion
  441.1 0.3 gather.7
  441.4 2.3 multiply_reduce_fusion
  443.8 0.8 add_convert_fusion
  (92 shorter events, 1.4 us)
Async XLA Ops:
  6.5 323.1 %copy-start = (bf16[1,128,2048]{2,1,0:T(8,128)(2,1)S(1)}, bf16[1,128,2048]{2,1,0:T(8,128)(2,1)}, u32[]{:S(2)}) copy-start(bf16[1,128,2048]{2,1,0:T(8,128)(2,1)} %param.37) | copy-start | bytes 1572868
  6.5 6.4 %copy-start.3 = (bf16[1024,512]{1,0:T(8,128)(2,1)S(1)}, bf16[1024,512]{1,0:T(8,128)(2,1)}, u32[]{:S(2)}) copy-start(bf16[1024,512]{1,0:T(8,128)(2,1)} %param.22) | copy-start | bytes 3145732
  6.5 6.5 %copy-start.12 = (f32[512]{0:T(512)S(1)}, f32[512]{0:T(512)}, u32[]{:S(2)}) copy-start(f32[512]{0:T(512)} %param.24) | copy-start | bytes 6148
  6.5 7.0 %copy-start.4 = (bf16[1024,96]{0,1:T(8,128)(2,1)S(1)}, bf16[1024,96]{0,1:T(8,128)(2,1)}, u32[]{:S(2)}) copy-start(bf16[1024,96]{0,1:T(8,128)(2,1)} %param.21) | copy-start | bytes 589828
  6.5 6.5 %copy-start.11 = (bf16[512,64]{0,1:T(8,128)(2,1)S(1)}, bf16[512,64]{0,1:T(8,128)(2,1)}, u32[]{:S(2)}) copy-start(bf16[512,64]{0,1:T(8,128)(2,1)} %param.26) | copy-start | bytes 196612
  6.5 7.0 %copy-start.10 = (f32[96]{0:T(128)S(1)}, f32[96]{0:T(128)}, u32[]{:S(2)}) copy-start(f32[96]{0:T(128)} %param.27) | copy-start | bytes 1156
  6.6 71.4 %all-gather.3.cloned.1.call-start = ((), (), s32[]{:S(2)}) async-start(), calls=%async_computation.4 | async-start | bytes 5570560 | tf_op jit(solution)/shard_map/all_gather | solution.py:114
  8.3 6.8 %copy-start.8 = (f32[1024]{0:T(1024)S(1)}, f32[1024]{0:T(1024)}, u32[]{:S(2)}) copy-start(f32[1024]{0:T(1024)} %param.29) | copy-start | bytes 12292
  8.3 6.9 %copy-start.6 = (s32[64,2]{0,1:T(2,128)S(1)}, s32[64,2]{0,1:T(2,128)}, u32[]{:S(2)}) copy-start(s32[64,2]{0,1:T(2,128)} %param.33) | copy-start | bytes 1540
  80.1 2.0 copy-start.1
  89.0 14.1 %all-to-all-start = ((bf16[16,2,2048]{2,1,0:T(2,128)(2,1)}), bf16[16,2,2048]{2,1,0:T(2,128)(2,1)S(1)}, u32[]{:S(2)}, u32[]{:S(2)}) async-start(bf16[16,2,2048]{2,1,0:T(2,128)(2,1)} %reshape.512), calls=%async_computation | async-start | bytes 262144 | tf_op jit(solution)/shard_map/all_to_all | solution.py:153
  96.8 227.5 %all-gather.5.cloned.1.call-start = ((), (), s32[]{:S(2)}) async-start(), calls=%async_computation.5 | async-start | bytes 10027008 | tf_op jit(solution)/shard_map/all_gather | solution.py:179
  107.0 1.0 copy-start.2
  107.0 1.1 copy-start.7
  266.8 62.8 %copy-start.5 = (bf16[1,2048,128]{2,1,0:T(8,128)(2,1)S(1)}, bf16[1,2048,128]{2,1,0:T(8,128)(2,1)}, u32[]{:S(2)}) copy-start(bf16[1,2048,128]{2,1,0:T(8,128)(2,1)} %param.36) | copy-start | bytes 1572868
  266.8 148.7 %reduce-scatter.2.cloned.1.call-start = ((), (), s32[]{:S(2)}) async-start(), calls=%async_computation.6 | async-start | bytes 10027008 | tf_op jit(solution)/shard_map/reduce_scatter | solution.py:183
  343.8 80.8 %copy-start.9 = (f32[64,2]{0,1:T(2,128)S(1)}, f32[64,2]{0,1:T(2,128)}, u32[]{:S(2)}) copy-start(f32[64,2]{0,1:T(2,128)} %param.34) | copy-start | bytes 1540
  417.8 22.1 %all-to-all-start.2 = ((bf16[16,9,2048]{2,1,0:T(8,128)(2,1)}), bf16[16,9,2048]{2,1,0:T(8,128)(2,1)S(1)}, u32[]{:S(2)}, u32[]{:S(2)}) async-start(bf16[16,9,2048]{2,1,0:T(8,128)(2,1)} %reshape.502), calls=%async_computation.3 | async-start | bytes 2097152 | tf_op jit(solution)/shard_map/all_to_all | solution.py:189
Sparse Core Ops, SparseCore 0:
  14.9 62.9 all-gather.2
  266.9 57.2 all-gather.4
  344.0 71.4 reduce-scatter.1
where the time goes:
time: 452 us; the launch traced here: 451 us
  waiting for transfers between devices  212 us (47%)
  blocking collectives  157 us (35%)
  matrix products  31.3 us (7%)
  starting transfers between devices  14.6 us (3%)
  between operations  13.5 us (3%)
  other arithmetic  12 us (3%)
  local copies, waits for them, and re-layouts  9.85 us (2%)
    all_to_all x1, blocking collectives, shards(): lax.all_to_all(outbound, 'sp', split_axis=0, concat_axis=0, tiled=True)  157 us
    reduce_scatter x1, waiting for transfers between devices, shards(): lax.psum_scatter(jnp.dot(hidden, expert_down[0], preferred_element_type=j...  71.6 us
    all_gather x1, waiting for transfers between devices, shards(): key_piece = lax.all_gather(bundle, 'sp', axis=2, tiled=True)  61.9 us
    all_gather x1, waiting for transfers between devices, shards(): row_block = lax.all_gather(flat_rows, 'tp', axis=0, tiled=True)  57.2 us
    all_to_all x1, waiting for transfers between devices, shards(): lax.all_to_all(served, 'sp', split_axis=0, concat_axis=0, tiled=True)  15.1 us
    dot_general x1, matrix products, shards(): jnp.dot(hidden, expert_down[0], preferred_element_type=jnp.float32)  14.2 us
  transfers between devices with their start and end apart: 5, of which 5 were waited for; matrix products, arithmetic and copies ran while one was open for 0% of the time, Pallas kernels for 0%

commit v1 on v0

--- a/solution.py
+++ b/solution.py
@@ -176,7 +176,16 @@
     arrived = lax.all_to_all(outbound, "sp", split_axis=0, concat_axis=0, tiled=True)
     item_count = arrived.shape[1]
     flat_rows = arrived.reshape(sp_count * item_count, D)
-    row_block = lax.all_gather(flat_rows, "tp", axis=0, tiled=True)
+    ways = lax.axis_size("tp")
+    up = [(d, (d + 1) % ways) for d in range(ways)]
+    down = [(d, (d - 1) % ways) for d in range(ways)]
+    earlier_2, later = ([flat_rows], [flat_rows])
+    for _ in range(ways // 2):
+        earlier_2.append(lax.ppermute(earlier_2[-1], "tp", up))
+    for _ in range((ways - 1) // 2):
+        later.append(lax.ppermute(later[-1], "tp", down))
+    line = jnp.concatenate([*earlier_2[::-1], *later[1:]], axis=0)
+    row_block = jnp.roll(line, (lax.axis_index("tp") - ways // 2) * flat_rows.shape[0], axis=0)
     gate_pre = jnp.dot(row_block, expert_gate[0], preferred_element_type=jnp.float32)
     up_pre = jnp.dot(row_block, expert_up[0], preferred_element_type=jnp.float32)
     hidden = (jax.nn.silu(gate_pre) * up_pre).astype(jnp.bfloat16)

time: 452 us -> 501 us (1.11)
  starting transfers between devices: 14.6 us -> 42.5 us
  local copies, waits for them, and re-layouts: 9.85 us -> 36.6 us
  waiting for transfers between devices: 212 us -> 205 us
    all_gather x1 -> x0, waiting for transfers between devices: 57.2 us -> none  [shards(): row_block = lax.all_gather(flat_rows, 'tp', axis=0, tiled=True)]
    ppermute x0 -> x15, waiting for transfers between devices: none -> 52.4 us  [the longest x8 47 us: shards(): earlier_2.append(lax.ppermute(earlier_2[-1], 'tp', up))]
    ppermute x0 -> x15, starting transfers between devices: none -> 28.1 us  [the longest x8 28.1 us: shards(): earlier_2.append(lax.ppermute(earlier_2[-1], 'tp', up))]
    unnamed x29 -> x80, local copies, waits for them, and re-layouts: 1.7 us -> 28.5 us
  transfers between devices with their start and end apart: 5 -> 19, of which waited for: 5 -> 16; matrix products, arithmetic and copies ran while one was open for 0% -> 3% of each run, Pallas kernels for 0% -> 0%
where the time goes in v1:
time: 501 us; the launch traced here: 499 us
  waiting for transfers between devices  205 us (41%)
  blocking collectives  157 us (31%)
  starting transfers between devices  42.5 us (8%)
  local copies, waits for them, and re-layouts  36.6 us (7%)
  matrix products  30.2 us (6%)
  between operations  14.1 us (3%)
  other arithmetic  12.9 us (3%)
    all_to_all x1, blocking collectives, shards(): lax.all_to_all(outbound, 'sp', split_axis=0, concat_axis=0, tiled=True)  157 us
    reduce_scatter x1, waiting for transfers between devices, shards(): lax.psum_scatter(jnp.dot(hidden, expert_down[0], preferred_element_type=j...  71.3 us
    all_gather x1, waiting for transfers between devices, shards(): key_piece = lax.all_gather(bundle, 'sp', axis=2, tiled=True)  60.5 us
    ppermute x8, waiting for transfers between devices, shards(): earlier_2.append(lax.ppermute(earlier_2[-1], 'tp', up))  47 us
    unnamed x80, local copies, waits for them, and re-layouts  28.5 us
    ppermute x8, starting transfers between devices, shards(): earlier_2.append(lax.ppermute(earlier_2[-1], 'tp', up))  28.1 us
    all_to_all x1, waiting for transfers between devices, shards(): lax.all_to_all(served, 'sp', split_axis=0, concat_axis=0, tiled=True)  15 us
    dot_general x1, matrix products, shards(): jnp.dot(hidden, expert_down[0], preferred_element_type=jnp.float32)  14.5 us
  transfers between devices with their start and end apart: 19, of which 16 were waited for; matrix products, arithmetic and copies ran while one was open for 3% of the time, Pallas kernels for 0%

profile of v1, /device:TPU:97, one launch (start us, length us, event | category | flops | bytes accessed | tf_op | source)
XLA Modules:
  0.0 499.4 jit_solution(3052412768450823033)
XLA Ops:
  6.6 1.6 fusion.24
  8.1 1.8 fusion.27
  12.8 1.8 fusion.28
  19.4 60.5 %all-gather.2.cloned.1.call-done = bf16[1,160,16384]{2,1,0:T(8,128)(2,1)} async-done(((bf16[1,160,1024]{2,1,0:T(8,128)(2,1)}), bf16[1,160,16384]{2,1,0:T(8,128)(2,1)}) %all-gather.2.cloned.1.call-update) | async-done | bytes 5242896 | tf_op jit(solution)/shard_map/all_gather | solution.py:114
  80.0 9.9 %while.18 = (s32[]{:T(128)}, f32[1,1024]{1,0:T(1,128)S(1)}, f32[1,1024]{1,0:T(1,128)S(1)}, f32[1,1024,64]{1,2,0:T(8,128)S(1)}, s32[]{:T(128)}, /*index=5*/bf16[1...) while((s32[]{:T(128)}, f32[1,1024]{1,0:T(1,128)S(1)}, ...), condition=%wide.region_8.9_spmd.clone, body=%wide.region_3.8_spmd.clone.sunk | while | flops 352456704 | bytes 30515560 | solution.py:149
  80.0 9.1 %conditional.3 = ((f32[1,1024]{1,0:T(1,128)S(1)}, f32[1,1024]{1,0:T(1,128)S(1)}, f32[1,1024,64]{1,2,0:T(8,128)S(1)})) conditional(s32[]{:T(128)} %convert_element_type.206, (f32[1,1024]{1,0:T(1,128)S(1)}, f32[1,1024]{1,0:T(1,128)S(1)}, f32[1,1024,64]{1,2,0:T(8,128)S(1)}) %tuple.54, (s32[]{:T(128)}, s32[]{:T(128)}, s32[]{:T(128)}, ...), branch_computations={%region_4.0_spmd, %region_5.7_spmd} | conditional | flops 352456704 | bytes 30511242 | solution.py:147
  80.1 2.0 fusion.2
  82.1 2.0 copy-done.1
  84.1 1.5 fusion.4
  85.7 3.5 fusion.10
  91.0 7.8 %all-to-all-start = ((bf16[16,2,2048]{2,1,0:T(2,128)(2,1)}), bf16[16,2,2048]{2,1,0:T(2,128)(2,1)S(1)}, u32[]{:S(2)}, u32[]{:S(2)}) async-start(bf16[16,2,2048]{2,1,0:T(2,128)(2,1)} %reshape.512), calls=%async_computation | async-start | bytes 262144 | tf_op jit(solution)/shard_map/all_to_all | solution.py:153
  98.9 6.2 %all-to-all-done = bf16[16,2,2048]{2,1,0:T(2,128)(2,1)S(1)} async-done(((bf16[16,2,2048]{2,1,0:T(2,128)(2,1)}), bf16[16,2,2048]{2,1,0:T(2,128)(2,1)S(1)}, u32[]{:S(2)}, u32[]{:S(2)}) %all-to-all-start) | async-done | bytes 131104 | tf_op jit(solution)/shard_map/all_to_all | solution.py:153
  105.5 3.5 convert_bitcast_fusion
  110.6 156.8 %all_to_all.23 = bf16[16,9,2048]{2,1,0:T(8,128)(2,1)S(1)} all-to-all(bf16[16,9,2048]{2,1,0:T(8,128)(2,1)S(1)} %reshape.500), channel_id=1, replica_groups=mesh['sp'=16,'tp'=16] {'sp'}, dimensions={0} | all-to-all | bytes 1179648 | tf_op jit(solution)/shard_map/all_to_all | solution.py:176
  267.7 2.2 collective-permute-start
  269.9 6.8 %collective-permute-done = bf16[144,2048]{1,0:T(8,128)(2,1)S(1)} collective-permute-done((bf16[144,2048]{1,0:T(8,128)(2,1)S(1)}, bf16[144,2048]{1,0:T(8,128)(2,1)S(1)}, u32[]{:S(2)}, u32[]{:S(2)}) %collective-permute-start) | collective-permute-done | bytes 589856 | tf_op jit(solution)/shard_map/ppermute | solution.py:184
  276.7 3.7 collective-permute-start.1
  280.4 6.8 %collective-permute-done.1 = bf16[144,2048]{1,0:T(8,128)(2,1)S(1)} collective-permute-done((bf16[144,2048]{1,0:T(8,128)(2,1)S(1)}, bf16[144,2048]{1,0:T(8,128)(2,1)S(1)}, u32[]{:S(2)}, u32[]{:S(2)}) %collective-permute-start.1) | collective-permute-done | bytes 589856 | tf_op jit(solution)/shard_map/ppermute | solution.py:184
  287.2 3.7 collective-permute-start.2
  290.9 6.8 %collective-permute-done.2 = bf16[144,2048]{1,0:T(8,128)(2,1)S(1)} collective-permute-done((bf16[144,2048]{1,0:T(8,128)(2,1)S(1)}, bf16[144,2048]{1,0:T(8,128)(2,1)S(1)}, u32[]{:S(2)}, u32[]{:S(2)}) %collective-permute-start.2) | collective-permute-done | bytes 589856 | tf_op jit(solution)/shard_map/ppermute | solution.py:184
  297.7 3.7 collective-permute-start.3
  302.3 6.0 %collective-permute-done.3 = bf16[144,2048]{1,0:T(8,128)(2,1)S(1)} collective-permute-done((bf16[144,2048]{1,0:T(8,128)(2,1)S(1)}, bf16[144,2048]{1,0:T(8,128)(2,1)S(1)}, u32[]{:S(2)}, u32[]{:S(2)}) %collective-permute-start.3) | collective-permute-done | bytes 589856 | tf_op jit(solution)/shard_map/ppermute | solution.py:184
  308.3 3.7 collective-permute-start.4
  313.6 5.1 %collective-permute-done.4 = bf16[144,2048]{1,0:T(8,128)(2,1)S(1)} collective-permute-done((bf16[144,2048]{1,0:T(8,128)(2,1)S(1)}, bf16[144,2048]{1,0:T(8,128)(2,1)S(1)}, u32[]{:S(2)}, u32[]{:S(2)}) %collective-permute-start.4) | collective-permute-done | bytes 589856 | tf_op jit(solution)/shard_map/ppermute | solution.py:184
  318.8 3.7 collective-permute-start.5
  324.1 5.2 %collective-permute-done.5 = bf16[144,2048]{1,0:T(8,128)(2,1)S(1)} collective-permute-done((bf16[144,2048]{1,0:T(8,128)(2,1)S(1)}, bf16[144,2048]{1,0:T(8,128)(2,1)S(1)}, u32[]{:S(2)}, u32[]{:S(2)}) %collective-permute-start.5) | collective-permute-done | bytes 589856 | tf_op jit(solution)/shard_map/ppermute | solution.py:184
  329.3 3.7 collective-permute-start.6
  333.0 1.7 collective-permute-done.12
  334.8 5.1 %collective-permute-done.6 = bf16[144,2048]{1,0:T(8,128)(2,1)} collective-permute-done((bf16[144,2048]{1,0:T(8,128)(2,1)S(1)}, bf16[144,2048]{1,0:T(8,128)(2,1)}, u32[]{:S(2)}, u32[]{:S(2)}) %collective-permute-start.6) | collective-permute-done | bytes 589856 | tf_op jit(solution)/shard_map/ppermute | solution.py:184
  339.8 3.8 collective-permute-start.7
  343.7 1.9 collective-permute-done.13
  345.6 5.2 %collective-permute-done.7 = bf16[144,2048]{1,0:T(8,128)(2,1)} collective-permute-done((bf16[144,2048]{1,0:T(8,128)(2,1)}, bf16[144,2048]{1,0:T(8,128)(2,1)}, u32[]{:S(2)}, u32[]{:S(2)}) %collective-permute-start.7) | collective-permute-done | bytes 589856 | tf_op jit(solution)/shard_map/ppermute | solution.py:184
  351.9 1.1 constant_dynamic-update-slice_fusion.30
  353.0 1.1 constant_dynamic-update-slice_fusion.29
  354.1 1.1 constant_dynamic-update-slice_fusion.28
  355.2 1.1 constant_dynamic-update-slice_fusion.27
  356.4 1.1 constant_dynamic-update-slice_fusion.26
  357.7 1.1 constant_dynamic-update-slice_fusion.21
  364.4 1.1 constant_dynamic-update-slice_fusion.14
  366.2 1.1 constant_dynamic-update-slice_fusion.2
  368.5 6.5 %copy-done.2 = bf16[4608,2048]{1,0:T(8,128)(2,1)} copy-done((bf16[4608,2048]{1,0:T(8,128)(2,1)}, bf16[4608,2048]{1,0:T(8,128)(2,1)S(1)}, u32[]{:S(2)}) %copy-start.2) | copy-done | bytes 18874392
  375.0 2.8 fusion.20
  377.8 14.5 %convolution_convert_fusion = bf16[2304,2048]{1,0:T(8,128)(2,1)} fusion(f32[2304,128]{1,0:T(8,128)S(1)} %fusion.20, bf16[4608,2048]{1,0:T(8,128)(2,1)} %copy-done.2, s32[]{:T(128)S(6)} %select_n.49, bf16[1,128,2048]{2,1,0:T(8,128)(2,1)S(1)} %copy-done, bf16[1,2048,128]{2,1,0:T(8,128)(2,1)} %param.35), kind=kOutput, calls=%fused_computation.23 | convolution fusion | flops 2422407168 | bytes 21102596 | tf_op jit(solution)/shard_map/dot_general | solution.py:193
  392.3 71.3 %reduce-scatter.2.cloned.1.call-done = bf16[144,2048]{1,0:T(8,128)(2,1)} async-done(((bf16[2304,2048]{1,0:T(8,128)(2,1)}), bf16[144,2048]{1,0:T(8,128)(2,1)}) %reduce-scatter.2.cloned.1.call-update) | async-done | bytes 589840 | tf_op jit(solution)/shard_map/reduce_scatter | solution.py:192
  463.6 2.3 reshape.502
  465.9 6.5 %all-to-all-start.2 = ((bf16[16,9,2048]{2,1,0:T(8,128)(2,1)}), bf16[16,9,2048]{2,1,0:T(8,128)(2,1)S(1)}, u32[]{:S(2)}, u32[]{:S(2)}) async-start(bf16[16,9,2048]{2,1,0:T(8,128)(2,1)} %reshape.502), calls=%async_computation.3 | async-start | bytes 2097152 | tf_op jit(solution)/shard_map/all_to_all | solution.py:198
  472.9 15.0 %all-to-all-done.2 = bf16[16,9,2048]{2,1,0:T(8,128)(2,1)S(1)} async-done(((bf16[16,9,2048]{2,1,0:T(8,128)(2,1)}), bf16[16,9,2048]{2,1,0:T(8,128)(2,1)S(1)}, u32[]{:S(2)}, u32[]{:S(2)}) %all-to-all-start.2) | async-done | bytes 589856 | tf_op jit(solution)/shard_map/all_to_all | solution.py:198
  489.4 2.3 multiply_reduce_fusion
  (171 shorter events, 26.8 us)
Async XLA Ops:
  6.5 371.2 %copy-start = (bf16[1,128,2048]{2,1,0:T(8,128)(2,1)S(1)}, bf16[1,128,2048]{2,1,0:T(8,128)(2,1)}, u32[]{:S(2)}) copy-start(bf16[1,128,2048]{2,1,0:T(8,128)(2,1)} %param.37) | copy-start | bytes 1572868
  6.5 73.4 %all-gather.2.cloned.1.call-start = ((), (), s32[]{:S(2)}) async-start(), calls=%async_computation.4 | async-start | bytes 5570560 | tf_op jit(solution)/shard_map/all_gather | solution.py:114
  80.0 18.9 %copy-start.19 = (s32[64,2]{0,1:T(2,128)S(1)}, s32[64,2]{0,1:T(2,128)}, u32[]{:S(2)}) copy-start(s32[64,2]{0,1:T(2,128)} %param.33) | copy-start | bytes 1540
  80.0 29.8 %copy-start.17 = (bf16[64,2048]{1,0:T(8,128)(2,1)S(1)}, bf16[64,2048]{1,0:T(8,128)(2,1)}, u32[]{:S(2)}) copy-start(bf16[64,2048]{1,0:T(8,128)(2,1)} %param.31) | copy-start | bytes 786436
  80.0 30.0 %copy-start.20 = (f32[2048]{0:T(1024)S(1)}, f32[2048]{0:T(1024)}, u32[]{:S(2)}) copy-start(f32[2048]{0:T(1024)} %param.32) | copy-start | bytes 24580
  82.1 2.0 copy-start.1
  91.0 14.1 %all-to-all-start = ((bf16[16,2,2048]{2,1,0:T(2,128)(2,1)}), bf16[16,2,2048]{2,1,0:T(2,128)(2,1)S(1)}, u32[]{:S(2)}, u32[]{:S(2)}) async-start(bf16[16,2,2048]{2,1,0:T(2,128)(2,1)} %reshape.512), calls=%async_computation | async-start | bytes 262144 | tf_op jit(solution)/shard_map/all_to_all | solution.py:153
  98.8 364.8 %reduce-scatter.2.cloned.1.call-start = ((), (), s32[]{:S(2)}) async-start(), calls=%async_computation.5 | async-start | bytes 10027008 | tf_op jit(solution)/shard_map/reduce_scatter | solution.py:192
  267.7 9.0 %collective-permute-start = (bf16[144,2048]{1,0:T(8,128)(2,1)S(1)}, bf16[144,2048]{1,0:T(8,128)(2,1)S(1)}, u32[]{:S(2)}, u32[]{:S(2)}) collective-permute-start(bf16[144,2048]{1,0:T(8,128)(2,1)S(1)} %reshape.501), channel_id=1, source_target_pairs={{0,1},{1,2},{2,3},{3,4},{4,5},{5,6},{6,7},{7,8},{8,9},{9,10},{10,1... | collective-permute-start | bytes 1769480 | tf_op jit(solution)/shard_map/ppermute | solution.py:184
  276.7 10.5 %collective-permute-start.1 = (bf16[144,2048]{1,0:T(8,128)(2,1)S(1)}, bf16[144,2048]{1,0:T(8,128)(2,1)S(1)}, u32[]{:S(2)}, u32[]{:S(2)}) collective-permute-start(bf16[144,2048]{1,0:T(8,128)(2,1)S(1)} %collective-permute-done), channel_id=1, source_target_pairs={{0,1},{1,2},{2,3},{3,4},{4,5},{5,6},{6,7},{7,8},{8,9},{9,10},{10,1... | collective-permute-start | bytes 1769480 | tf_op jit(solution)/shard_map/ppermute | solution.py:184
  280.4 10.5 %collective-permute-start.8 = (bf16[144,2048]{1,0:T(8,128)(2,1)S(1)}, bf16[144,2048]{1,0:T(8,128)(2,1)S(1)}, u32[]{:S(2)}, u32[]{:S(2)}) collective-permute-start(bf16[144,2048]{1,0:T(8,128)(2,1)S(1)} %reshape.501), channel_id=1, source_target_pairs={{0,15},{1,0},{2,1},{3,2},{4,3},{5,4},{6,5},{7,6},{8,7},{9,8},{10,9... | collective-permute-start | bytes 1769480 | tf_op jit(solution)/shard_map/ppermute | solution.py:186
  287.2 10.5 %collective-permute-start.2 = (bf16[144,2048]{1,0:T(8,128)(2,1)S(1)}, bf16[144,2048]{1,0:T(8,128)(2,1)S(1)}, u32[]{:S(2)}, u32[]{:S(2)}) collective-permute-start(bf16[144,2048]{1,0:T(8,128)(2,1)S(1)} %collective-permute-done.1), channel_id=1, source_target_pairs={{0,1},{1,2},{2,3},{3,4},{4,5},{5,6},{6,7},{7,8},{8,9},{9,10},{10,1... | collective-permute-start | bytes 1769480 | tf_op jit(solution)/shard_map/ppermute | solution.py:184
  290.9 10.5 %collective-permute-start.9 = (bf16[144,2048]{1,0:T(8,128)(2,1)S(1)}, bf16[144,2048]{1,0:T(8,128)(2,1)S(1)}, u32[]{:S(2)}, u32[]{:S(2)}) collective-permute-start(bf16[144,2048]{1,0:T(8,128)(2,1)S(1)} %collective-permute-done.8), channel_id=1, source_target_pairs={{0,15},{1,0},{2,1},{3,2},{4,3},{5,4},{6,5},{7,6},{8,7},{9,8},{10,9... | collective-permute-start | bytes 1769480 | tf_op jit(solution)/shard_map/ppermute | solution.py:186
  297.7 15.0 %copy-start.5 = (bf16[144,2048]{1,0:T(8,128)(2,1)}, bf16[144,2048]{1,0:T(8,128)(2,1)S(1)}, u32[]{:S(2)}) copy-start(bf16[144,2048]{1,0:T(8,128)(2,1)S(1)} %collective-permute-done.2) | copy-start | bytes 1769476
  297.7 10.5 %collective-permute-start.3 = (bf16[144,2048]{1,0:T(8,128)(2,1)S(1)}, bf16[144,2048]{1,0:T(8,128)(2,1)S(1)}, u32[]{:S(2)}, u32[]{:S(2)}) collective-permute-start(bf16[144,2048]{1,0:T(8,128)(2,1)S(1)} %collective-permute-done.2), channel_id=1, source_target_pairs={{0,1},{1,2},{2,3},{3,4},{4,5},{5,6},{6,7},{7,8},{8,9},{9,10},{10,1... | collective-permute-start | bytes 1769480 | tf_op jit(solution)/shard_map/ppermute | solution.py:184
  301.4 0.8 copy-start.3
  302.3 10.5 %collective-permute-start.10 = (bf16[144,2048]{1,0:T(8,128)(2,1)S(1)}, bf16[144,2048]{1,0:T(8,128)(2,1)S(1)}, u32[]{:S(2)}, u32[]{:S(2)}) collective-permute-start(bf16[144,2048]{1,0:T(8,128)(2,1)S(1)} %collective-permute-done.9), channel_id=1, source_target_pairs={{0,15},{1,0},{2,1},{3,2},{4,3},{5,4},{6,5},{7,6},{8,7},{9,8},{10,9... | collective-permute-start | bytes 1769480 | tf_op jit(solution)/shard_map/ppermute | solution.py:186
  308.3 26.5 %copy-start.11 = (bf16[144,2048]{1,0:T(8,128)(2,1)}, bf16[144,2048]{1,0:T(8,128)(2,1)S(1)}, u32[]{:S(2)}) copy-start(bf16[144,2048]{1,0:T(8,128)(2,1)S(1)} %collective-permute-done.3) | copy-start | bytes 1769476
  308.3 10.5 %collective-permute-start.4 = (bf16[144,2048]{1,0:T(8,128)(2,1)S(1)}, bf16[144,2048]{1,0:T(8,128)(2,1)S(1)}, u32[]{:S(2)}, u32[]{:S(2)}) collective-permute-start(bf16[144,2048]{1,0:T(8,128)(2,1)S(1)} %collective-permute-done.3), channel_id=1, source_target_pairs={{0,1},{1,2},{2,3},{3,4},{4,5},{5,6},{6,7},{7,8},{8,9},{9,10},{10,1... | collective-permute-start | bytes 1769480 | tf_op jit(solution)/shard_map/ppermute | solution.py:184
  312.8 0.9 copy-start.7
  312.8 10.5 %collective-permute-start.11 = (bf16[144,2048]{1,0:T(8,128)(2,1)S(1)}, bf16[144,2048]{1,0:T(8,128)(2,1)S(1)}, u32[]{:S(2)}, u32[]{:S(2)}) collective-permute-start(bf16[144,2048]{1,0:T(8,128)(2,1)S(1)} %collective-permute-done.10), channel_id=1, source_target_pairs={{0,15},{1,0},{2,1},{3,2},{4,3},{5,4},{6,5},{7,6},{8,7},{9,8},{10,9... | collective-permute-start | bytes 1769480 | tf_op jit(solution)/shard_map/ppermute | solution.py:186
  318.8 16.0 %copy-start.13 = (bf16[144,2048]{1,0:T(8,128)(2,1)}, bf16[144,2048]{1,0:T(8,128)(2,1)S(1)}, u32[]{:S(2)}) copy-start(bf16[144,2048]{1,0:T(8,128)(2,1)S(1)} %collective-permute-done.4) | copy-start | bytes 1769476
  318.8 10.5 %collective-permute-start.5 = (bf16[144,2048]{1,0:T(8,128)(2,1)S(1)}, bf16[144,2048]{1,0:T(8,128)(2,1)S(1)}, u32[]{:S(2)}, u32[]{:S(2)}) collective-permute-start(bf16[144,2048]{1,0:T(8,128)(2,1)S(1)} %collective-permute-done.4), channel_id=1, source_target_pairs={{0,1},{1,2},{2,3},{3,4},{4,5},{5,6},{6,7},{7,8},{8,9},{9,10},{10,1... | collective-permute-start | bytes 1769480 | tf_op jit(solution)/shard_map/ppermute | solution.py:184
  323.3 0.8 copy-start.9
  324.1 10.6 %collective-permute-start.12 = (bf16[144,2048]{1,0:T(8,128)(2,1)S(1)}, bf16[144,2048]{1,0:T(8,128)(2,1)}, u32[]{:S(2)}, u32[]{:S(2)}) collective-permute-start(bf16[144,2048]{1,0:T(8,128)(2,1)S(1)} %collective-permute-done.11), channel_id=1, source_target_pairs={{0,15},{1,0},{2,1},{3,2},{4,3},{5,4},{6,5},{7,6},{8,7},{9,8},{10,9... | collective-permute-start | bytes 1769480 | tf_op jit(solution)/shard_map/ppermute | solution.py:186
  329.3 10.5 %copy-start.15 = (bf16[144,2048]{1,0:T(8,128)(2,1)}, bf16[144,2048]{1,0:T(8,128)(2,1)S(1)}, u32[]{:S(2)}) copy-start(bf16[144,2048]{1,0:T(8,128)(2,1)S(1)} %collective-permute-done.5) | copy-start | bytes 1769476
  329.3 10.5 %collective-permute-start.6 = (bf16[144,2048]{1,0:T(8,128)(2,1)S(1)}, bf16[144,2048]{1,0:T(8,128)(2,1)}, u32[]{:S(2)}, u32[]{:S(2)}) collective-permute-start(bf16[144,2048]{1,0:T(8,128)(2,1)S(1)} %collective-permute-done.5), channel_id=1, source_target_pairs={{0,1},{1,2},{2,3},{3,4},{4,5},{5,6},{6,7},{7,8},{8,9},{9,10},{10,1... | collective-permute-start | bytes 1769480 | tf_op jit(solution)/shard_map/ppermute | solution.py:184
  334.8 10.8 %collective-permute-start.13 = (bf16[144,2048]{1,0:T(8,128)(2,1)}, bf16[144,2048]{1,0:T(8,128)(2,1)}, u32[]{:S(2)}, u32[]{:S(2)}) collective-permute-start(bf16[144,2048]{1,0:T(8,128)(2,1)} %collective-permute-done.12), channel_id=1, source_target_pairs={{0,15},{1,0},{2,1},{3,2},{4,3},{5,4},{6,5},{7,6},{8,7},{9,8},{10,9... | collective-permute-start | bytes 1769480 | tf_op jit(solution)/shard_map/ppermute | solution.py:186
  339.8 10.9 %collective-permute-start.7 = (bf16[144,2048]{1,0:T(8,128)(2,1)}, bf16[144,2048]{1,0:T(8,128)(2,1)}, u32[]{:S(2)}, u32[]{:S(2)}) collective-permute-start(bf16[144,2048]{1,0:T(8,128)(2,1)} %collective-permute-done.6), channel_id=1, source_target_pairs={{0,1},{1,2},{2,3},{3,4},{4,5},{5,6},{6,7},{7,8},{8,9},{9,10},{10,1... | collective-permute-start | bytes 1769480 | tf_op jit(solution)/shard_map/ppermute | solution.py:184
  343.6 21.9 %copy-start.16 = (bf16[144,2048]{1,0:T(8,128)(2,1)S(1)}, bf16[144,2048]{1,0:T(8,128)(2,1)}, u32[]{:S(2)}) copy-start(bf16[144,2048]{1,0:T(8,128)(2,1)} %copy-done.15) | copy-start | bytes 1769476
  343.6 22.0 %copy-start.14 = (bf16[144,2048]{1,0:T(8,128)(2,1)S(1)}, bf16[144,2048]{1,0:T(8,128)(2,1)}, u32[]{:S(2)}) copy-start(bf16[144,2048]{1,0:T(8,128)(2,1)} %copy-done.13) | copy-start | bytes 1769476
  343.6 22.0 %copy-start.12 = (bf16[144,2048]{1,0:T(8,128)(2,1)S(1)}, bf16[144,2048]{1,0:T(8,128)(2,1)}, u32[]{:S(2)}) copy-start(bf16[144,2048]{1,0:T(8,128)(2,1)} %copy-done.11) | copy-start | bytes 1769476
  343.6 22.1 %copy-start.6 = (bf16[144,2048]{1,0:T(8,128)(2,1)S(1)}, bf16[144,2048]{1,0:T(8,128)(2,1)}, u32[]{:S(2)}) copy-start(bf16[144,2048]{1,0:T(8,128)(2,1)} %copy-done.5) | copy-start | bytes 1769476
  343.6 22.4 %copy-start.4 = (bf16[144,2048]{1,0:T(8,128)(2,1)S(1)}, bf16[144,2048]{1,0:T(8,128)(2,1)}, u32[]{:S(2)}) copy-start(bf16[144,2048]{1,0:T(8,128)(2,1)} %copy-done.3) | copy-start | bytes 1769476
  343.7 22.4 %copy-start.8 = (bf16[144,2048]{1,0:T(8,128)(2,1)S(1)}, bf16[144,2048]{1,0:T(8,128)(2,1)}, u32[]{:S(2)}) copy-start(bf16[144,2048]{1,0:T(8,128)(2,1)} %copy-done.7) | copy-start | bytes 1769476
  343.7 22.5 %copy-start.10 = (bf16[144,2048]{1,0:T(8,128)(2,1)S(1)}, bf16[144,2048]{1,0:T(8,128)(2,1)}, u32[]{:S(2)}) copy-start(bf16[144,2048]{1,0:T(8,128)(2,1)} %copy-done.9) | copy-start | bytes 1769476
  343.7 31.3 %copy-start.22 = (bf16[1,2048,128]{2,1,0:T(8,128)(2,1)S(1)}, bf16[1,2048,128]{2,1,0:T(8,128)(2,1)}, u32[]{:S(2)}) copy-start(bf16[1,2048,128]{2,1,0:T(8,128)(2,1)} %param.36) | copy-start | bytes 1572868
  345.6 17.7 %collective-permute-start.14 = (bf16[144,2048]{1,0:T(8,128)(2,1)}, bf16[144,2048]{1,0:T(8,128)(2,1)S(1)}, u32[]{:S(2)}, u32[]{:S(2)}) collective-permute-start(bf16[144,2048]{1,0:T(8,128)(2,1)} %collective-permute-done.13), channel_id=1, source_target_pairs={{0,15},{1,0},{2,1},{3,2},{4,3},{5,4},{6,5},{7,6},{8,7},{9,8},{10,9... | collective-permute-start | bytes 1769480 | tf_op jit(solution)/shard_map/ppermute | solution.py:186
  368.5 6.5 %copy-start.2 = (bf16[4608,2048]{1,0:T(8,128)(2,1)}, bf16[4608,2048]{1,0:T(8,128)(2,1)S(1)}, u32[]{:S(2)}) copy-start(bf16[4608,2048]{1,0:T(8,128)(2,1)S(1)} %constant_dynamic-update-slice_fusion) | copy-start | bytes 56623108
  377.7 95.0 %copy-start.21 = (f32[64,2]{0,1:T(2,128)S(1)}, f32[64,2]{0,1:T(2,128)}, u32[]{:S(2)}) copy-start(f32[64,2]{0,1:T(2,128)} %param.34) | copy-start | bytes 1540
  377.7 114.0 %copy-start.18 = (bf16[64,2048]{1,0:T(8,128)(2,1)S(1)}, bf16[64,2048]{1,0:T(8,128)(2,1)}, u32[]{:S(2)}) copy-start(bf16[64,2048]{1,0:T(8,128)(2,1)} %param.31) | copy-start | bytes 786436
  465.9 22.0 %all-to-all-start.2 = ((bf16[16,9,2048]{2,1,0:T(8,128)(2,1)}), bf16[16,9,2048]{2,1,0:T(8,128)(2,1)S(1)}, u32[]{:S(2)}, u32[]{:S(2)}) async-start(bf16[16,9,2048]{2,1,0:T(8,128)(2,1)} %reshape.502), calls=%async_computation.3 | async-start | bytes 2097152 | tf_op jit(solution)/shard_map/all_to_all | solution.py:198
Sparse Core Ops, SparseCore 0:
  16.9 62.9 all-gather.1
  392.4 71.1 reduce-scatter.1
